TPU v7x, 32 devices: a whole 2x2x4 slice. The times are simulated.
32 devices in a mesh: ep: 16 (over z, y, x), tp: 2 (over core).
Axes of the slice: x: 2, y: 2, z: 4, core: 2. Of those that a mesh axis runs over, the one named last changes fastest.
Arguments:
- tokens: bfloat16 [1024, 2048], P('ep', 'tp'), may hold values from -6 to 6
- sequence_state_real: float32 [1024, 128, 64], P('ep', 'tp'), may hold values from -4 to 4
- sequence_state_imaginary: float32 [1024, 128, 64], P('ep', 'tp'), may hold values from -4 to 4
- mixer_norm_gain: float32 [2048], replicated, may hold values from 0.1 to 1.9
- expert_norm_gain: float32 [2048], replicated, may hold values from 0.1 to 1.9
- rate: float32 [128, 64], P('tp'), may hold values from 0.1 to 4
- freq: float32 [128, 64], P('tp'), may hold values from -3 to 3
- log_group_step: float32 [128], P('tp'), may hold values from -3 to 0
- input_map_real: float32 [128, 64, 16], P('tp'), may hold values from -1 to 1
- input_map_imaginary: float32 [128, 64, 16], P('tp'), may hold values from -1 to 1
- output_map_real: float32 [128, 16, 64], P('tp'), may hold values from -0.75 to 0.75
- output_map_imaginary: float32 [128, 16, 64], P('tp'), may hold values from -0.75 to 0.75
- skip: float32 [2048], P('tp'), may hold values from -4 to 4
- mixer_value_weight: bfloat16 [2048, 2048], P('tp'), may hold values from -0.125 to 0.125
- mixer_gate_weight: bfloat16 [2048, 2048], P('tp'), may hold values from -0.125 to 0.125
- group_router_weight: bfloat16 [2048, 4], replicated, may hold values from -0.125 to 0.125
- expert_router_weight: bfloat16 [2048, 16], replicated, may hold values from -0.125 to 0.125
- dense_blend_weight: float32 [2048], replicated, may hold values from -0.125 to 0.125
- routes: int32 [1024, 2], P('ep'), may hold values from 0 to 15, all different within a row; in each aligned block of 64 rows (0 to 63, 64 to 127, ...) at most 16 rows name the same one
- expert_gate_weight: bfloat16 [16, 2048, 1024], P('ep', None, 'tp'), may hold values from -0.125 to 0.125
- expert_up_weight: bfloat16 [16, 2048, 1024], P('ep', None, 'tp'), may hold values from -0.125 to 0.125
- expert_down_weight: bfloat16 [16, 1024, 2048], P('ep', 'tp'), may hold values from -0.1875 to 0.1875
- shared_gate_weight: bfloat16 [2048, 2048], P('tp', 'ep'), may hold values from -0.125 to 0.125
- shared_up_weight: bfloat16 [2048, 2048], P('tp', 'ep'), may hold values from -0.125 to 0.125
- shared_down_weight: bfloat16 [2048, 2048], P(None, 'tp'), may hold values from -0.125 to 0.125
Outputs:
- result: bfloat16 [1024, 2048], P('ep', 'tp')
- next_re: float32 [1024, 128, 64], P('ep', 'tp')
- next_im: float32 [1024, 128, 64], P('ep', 'tp')
Inputs may be any that keep to these rules, and one draw needn't show every extreme that they name: `routes`: each row names 2 different experts. Among the rows of one device no expert is named more than 16 times, and in every draw some expert is named exactly 16 times by some device's rows.
All inputs are finite; a program needn't handle non-finite values.
Results may differ from a plain program's by a relative error of at most 0.017.
Values may be sent and summed in bfloat16 or wider, within the bound.
A program may use at most 128 MiB of HBM per device.

v0:
```python
import jax
import jax.numpy as jnp
from jax import lax
from jax.sharding import PartitionSpec as P

NG = 4
EPS = 1e-06
PRECISION_MAX = lax.Precision.HIGHEST


def state_factors(rate, freq, log_group_step, input_map_real, input_map_imaginary):
    step_size = jnp.exp(log_group_step)[:, None]
    magnitude = jnp.exp(-rate * step_size)
    abar_re = magnitude * jnp.cos(freq * step_size)
    abar_im = magnitude * jnp.sin(freq * step_size)
    denom = rate * rate + freq * freq
    shift_re = abar_re - 1.0
    fac_re = (abar_im * freq - shift_re * rate) / denom
    fac_im = -(abar_im * rate + shift_re * freq) / denom
    bbar_re = fac_re[:, :, None] * input_map_real - fac_im[:, :, None] * input_map_imaginary
    bbar_im = fac_re[:, :, None] * input_map_imaginary + fac_im[:, :, None] * input_map_real
    return (abar_re, abar_im, bbar_re, bbar_im)


def state_step(
    normed,
    sequence_state_real,
    sequence_state_imaginary,
    factors,
    output_map_real,
    output_map_imaginary,
    skip,
):
    abar_re, abar_im, bbar_re, bbar_im = factors
    groups = abar_re.shape[0]
    inputs = normed.astype(jnp.float32)
    grouped = inputs.reshape(inputs.shape[0], groups, -1)
    drive_re = jnp.einsum("tgc,gpc->tgp", grouped, bbar_re, precision=PRECISION_MAX)
    drive_im = jnp.einsum("tgc,gpc->tgp", grouped, bbar_im, precision=PRECISION_MAX)
    fresh_real = abar_re * sequence_state_real - abar_im * sequence_state_imaginary + drive_re
    fresh_imaginary = abar_re * sequence_state_imaginary + abar_im * sequence_state_real + drive_im
    state_readout = jnp.einsum("dor,zdr->zdo", output_map_real, fresh_real, precision=PRECISION_MAX)
    state_readout = state_readout - jnp.einsum(
        "dor,zdr->zdo", output_map_imaginary, fresh_imaginary, precision=PRECISION_MAX
    )
    mixed = state_readout.reshape(inputs.shape) + skip * inputs
    return (mixed, fresh_real, fresh_imaginary)


def pair_product(left, first_map, second_map):
    first = jnp.dot(left, first_map, preferred_element_type=jnp.float32)
    second = jnp.dot(left, second_map, preferred_element_type=jnp.float32)
    return jnp.concatenate([first, second], axis=1)


def shards(
    tokens,
    sequence_state_real,
    sequence_state_imaginary,
    mixer_norm_gain,
    expert_norm_gain,
    rate,
    freq,
    log_group_step,
    input_map_real,
    input_map_imaginary,
    output_map_real,
    output_map_imaginary,
    skip,
    mixer_value_weight,
    mixer_gate_weight,
    group_router_weight,
    expert_router_weight,
    dense_blend_weight,
    routes,
    expert_gate_weight,
    expert_up_weight,
    expert_down_weight,
    shared_gate_weight,
    shared_up_weight,
    shared_down_weight,
):
    seq_rows, half_width = tokens.shape
    width = 2 * half_width
    column_start = lax.axis_index("tp") * half_width

    def own_rows(values):
        return lax.dynamic_slice_in_dim(values, column_start, half_width, 0)

    float_tokens = tokens.astype(jnp.float32)
    square_sum = lax.psum(jnp.sum(float_tokens * float_tokens, axis=1), "tp")
    first_scale = lax.rsqrt(square_sum / width + EPS)[:, None]
    normed = (float_tokens * first_scale * own_rows(mixer_norm_gain)).astype(jnp.bfloat16)
    factors = state_factors(rate, freq, log_group_step, input_map_real, input_map_imaginary)
    mixed, next_re, next_im = state_step(
        normed,
        sequence_state_real,
        sequence_state_imaginary,
        factors,
        output_map_real,
        output_map_imaginary,
        skip,
    )
    activated = jax.nn.gelu(mixed).astype(jnp.bfloat16)
    value_part = jnp.dot(activated, mixer_value_weight, preferred_element_type=jnp.float32)
    gate_part = jnp.dot(activated, mixer_gate_weight, preferred_element_type=jnp.float32)
    stacked = jnp.stack([value_part, gate_part], axis=1)
    mix_sum = lax.psum_scatter(
        stacked.astype(jnp.bfloat16), "tp", scatter_dimension=2, tiled=True
    ).astype(jnp.float32)
    mix_half = (mix_sum[:, 0] * jax.nn.sigmoid(mix_sum[:, 1])).astype(jnp.bfloat16)
    hidden = (float_tokens + mix_half.astype(jnp.float32)).astype(jnp.bfloat16)
    hidden_f32 = hidden.astype(jnp.float32)
    scaled = hidden_f32 * own_rows(expert_norm_gain)
    router_map = jnp.concatenate(
        [own_rows(group_router_weight), own_rows(expert_router_weight)], axis=1
    ).astype(jnp.float32)
    blend_map = own_rows(dense_blend_weight)
    hidden_squares = jnp.sum(hidden_f32 * hidden_f32, axis=1)
    total_squares = lax.psum(hidden_squares, "tp")
    inverse = lax.rsqrt(total_squares / width + EPS)[:, None]
    normal_rows = scaled * inverse
    raw_part = jnp.dot(normal_rows, router_map, precision=PRECISION_MAX)
    blend_part = jnp.dot(normal_rows, blend_map, precision=PRECISION_MAX)
    logits, blend_logit = lax.psum((raw_part, blend_part), "tp")
    hnorm = (scaled * inverse).astype(jnp.bfloat16)
    experts = expert_router_weight.shape[1]
    top_count = routes.shape[1]
    per_group = experts // NG
    group_prob = jax.nn.softmax(logits[:, :NG], axis=-1)
    expert_logits = logits[:, NG:]
    expert_hits = routes[:, :, None] == jnp.arange(experts, dtype=jnp.int32)[None, None, :]
    chosen = jnp.sum(jnp.where(expert_hits, expert_logits[:, None, :], 0.0), axis=2)
    group_hits = (routes // per_group)[:, :, None] == jnp.arange(NG, dtype=jnp.int32)[None, None, :]
    group_sel = jnp.sum(jnp.where(group_hits, group_prob[:, None, :], 0.0), axis=2)
    weights = jax.nn.softmax(chosen, axis=1) * group_sel
    full_rows = lax.all_gather(hnorm, "tp", axis=1, tiled=True)
    capacity = max(2, 2 * seq_rows * top_count // experts)
    flat_routes = routes.reshape(-1)
    matches = (flat_routes[:, None] == jnp.arange(experts, dtype=jnp.int32)[None, :]).astype(
        jnp.int32
    )
    slot_rank = jnp.sum(jnp.cumsum(matches, axis=0) * matches, axis=1) - 1
    slot_target = flat_routes * capacity + slot_rank
    dispatch = slot_target[None, :] == jnp.arange(experts * capacity, dtype=jnp.int32)[:, None]
    dispatch_rows = jnp.sum(
        dispatch.reshape(experts * capacity, seq_rows, top_count).astype(jnp.float32), axis=2
    )
    outgoing = jnp.dot(
        dispatch_rows.astype(jnp.bfloat16), full_rows, preferred_element_type=jnp.float32
    )
    outgoing = outgoing.astype(jnp.bfloat16).reshape(experts, capacity, width)
    received = lax.all_to_all(outgoing, "ep", split_axis=0, concat_axis=0, tiled=True)
    sources = received.shape[0]
    items = received.shape[1]
    token_rows = received.reshape(sources * items, width)
    gate_e = jnp.dot(token_rows, expert_gate_weight[0], preferred_element_type=jnp.float32)
    expert_up_rows = jnp.dot(token_rows, expert_up_weight[0], preferred_element_type=jnp.float32)
    inner = (jax.nn.silu(gate_e) * expert_up_rows).astype(jnp.bfloat16)
    part_out = jnp.dot(inner, expert_down_weight[0], preferred_element_type=jnp.float32)
    total = lax.psum_scatter(part_out.astype(jnp.bfloat16), "tp", scatter_dimension=1, tiled=True)
    finished = total.reshape(sources, items, half_width)
    returned = lax.all_to_all(finished, "ep", split_axis=0, concat_axis=0, tiled=True)
    returned_flat = returned.reshape(experts * capacity, half_width)
    picked = returned_flat[slot_target].reshape(seq_rows, top_count, half_width).astype(jnp.float32)
    routed = jnp.sum(weights[:, :, None] * picked, axis=1)
    partial_dense = pair_product(
        lax.all_gather(hnorm, "ep", axis=0, tiled=True), shared_gate_weight, shared_up_weight
    )
    dense_sum = lax.psum(partial_dense.astype(jnp.bfloat16), "tp").astype(jnp.float32)
    dense_cols = shared_gate_weight.shape[1]
    inner_cols = (jax.nn.silu(dense_sum[:, :dense_cols]) * dense_sum[:, dense_cols:]).astype(
        jnp.bfloat16
    )
    dense_inner = lax.all_to_all(inner_cols, "ep", split_axis=0, concat_axis=1, tiled=True)
    dense_out = jnp.dot(dense_inner, shared_down_weight, preferred_element_type=jnp.float32)
    result = hidden_f32 + routed + jax.nn.sigmoid(blend_logit)[:, None] * dense_out
    return (result.astype(jnp.bfloat16), next_re, next_im)


def solution(mesh):
    placed = (
        P("ep", "tp"),
        P("ep", "tp", None),
        P("ep", "tp", None),
        P(),
        P(),
        P("tp", None),
        P("tp", None),
        P("tp"),
        P("tp", None, None),
        P("tp", None, None),
        P("tp", None, None),
        P("tp", None, None),
        P("tp"),
        P("tp", None),
        P("tp", None),
        P(),
        P(),
        P(),
        P("ep", None),
        P("ep", None, "tp"),
        P("ep", None, "tp"),
        P("ep", "tp", None),
        P("tp", "ep"),
        P("tp", "ep"),
        P(None, "tp"),
    )
    return jax.shard_map(
        shards,
        mesh=mesh,
        in_specs=placed,
        out_specs=(P("ep", "tp"), P("ep", "tp", None), P("ep", "tp", None)),
        check_vma=False,
    )
```

profile of v0, /device:TPU:0, one launch (start us, length us, event | category | flops | bytes accessed | tf_op | source)
XLA Modules:
  0.0 187.7 jit_solution(3510667995029894204)
XLA Ops:
  7.2 3.5 %copy.64 = f32[64,64,64]{0,2,1:T(8,128)} copy(f32[64,64,64]{2,1,0:T(8,128)} %param.27) | data formatting | bytes 2097152 | tf_op args[2]
  10.7 3.4 %copy.63 = f32[64,64,64]{0,2,1:T(8,128)} copy(f32[64,64,64]{2,1,0:T(8,128)} %param.26) | data formatting | bytes 2097152 | tf_op args[1]
  14.3 2.6 %psum.35 = f32[64]{0:T(128)S(1)} all-reduce(f32[64]{0:T(128)S(1)} %fusion.29), channel_id=1, replica_groups=mesh['ep'=16,'tp'=2] {'tp'}, use_global_device_ids=true, to_apply=%region_1.0 | all-reduce | flops 64 | bytes 512 | tf_op jit(solution)/shard_map/psum | solution.py:91
  17.7 1.1 copy.65
  18.8 1.0 fusion.68
  19.8 4.9 %bitcast_add_fusion.1 = f32[64,64,64]{0,2,1:T(8,128)S(1)} fusion(f32[64,64,64]{0,2,1:T(8,128)} %copy.64, f32[64,64,64]{0,2,1:T(8,128)} %copy.63, bf16[64,64,16]{0,2,1:T(8,128)(2,1)S(1)} %bitcast.75, f32[64,64]{1,0:T(8,128)S(1)} %get-tuple-element.17, f32[64,64]{1,0:T(8,128)S(1)} %get-tuple-element.18, f32[64,64,16]{1,2,0:T(8,128)S(1)} %copy-done.7, ...), kind=kOutput, calls=%fused_computation.13 | convolution fusion | flops 51576832 | bytes 3866624 | tf_op jit(solution)/shard_map/tgc,gpc->tgp/dot_general | solution.py:38
  24.8 3.2 %bitcast_add_fusion = f32[64,64,64]{0,2,1:T(8,128)S(1)} fusion(f32[64,64,64]{0,2,1:T(8,128)S(1)} %copy-done.4, f32[64,64,64]{0,2,1:T(8,128)S(1)} %copy-done.3, bf16[64,64,16]{0,2,1:T(8,128)(2,1)S(1)} %bitcast.76, f32[64,64]{1,0:T(8,128)S(1)} %get-tuple-element.17, f32[64,64]{1,0:T(8,128)S(1)} %get-tuple-element.18, f32[64,64,16]{1,2,0:T(8,128)S(1)} %copy-done.8, ...), kind=kOutput, calls=%fused_computation.12 | convolution fusion | flops 51576832 | bytes 3866624 | tf_op jit(solution)/shard_map/tgc,gpc->tgp/dot_general | solution.py:39
  28.1 1.9 %fusion.77 = f32[64,64,16]{1,2,0:T(8,128)S(1)} fusion(f32[64,64,64]{0,2,1:T(8,128)S(1)} %bitcast_add_fusion.1, f32[64,16,64]{2,1,0:T(8,128)S(1)} %copy-done.11), kind=kOutput, calls=%fused_computation.123 | convolution fusion | flops 50331648 | bytes 1572864 | tf_op jit(solution)/shard_map/dor,zdr->zdo/dot_general | solution.py:42
  30.0 1.9 %convolution_subtract_fusion = f32[64,64,16]{1,2,0:T(8,128)S(1)} fusion(f32[64,64,16]{1,2,0:T(8,128)S(1)} %fusion.77, f32[64,64,64]{0,2,1:T(8,128)S(1)} %bitcast_add_fusion, f32[64,16,64]{2,1,0:T(8,128)S(1)} %copy-done.10), kind=kOutput, calls=%fused_computation.15 | convolution fusion | flops 50397184 | bytes 1835008 | tf_op jit(solution)/shard_map/dor,zdr->zdo/dot_general | solution.py:43
  32.1 3.3 %fusion.1 = bf16[64,1,2048]{2,0,1:T(8,128)(2,1)S(1)} fusion(bf16[1024,2048]{1,0:T(8,128)(2,1)} %param.39, f32[64,1024]{1,0:T(8,128)S(1)} %copy.70, f32[1024]{0:T(1024)S(1)} %copy-done.14, f32[1024]{0:T(1024)S(1)} %dynamic_slice.15, f32[64]{0:T(128)S(1)} %add_rsqrt_fusion.1, bf16[64,1024]{1,0:T(8,128)(2,1)S(1)} %copy-done.6), kind=kOutput, calls=%fused_computation.6 | convolution fusion | flops 269615104 | bytes 4858112 | tf_op jit(solution)/shard_map/dot_general | solution.py:106
  35.6 1.0 fusion
  37.8 10.3 %reduce-scatter.3.cloned.1.call-done = bf16[64,2,1024]{2,0,1:T(8,128)(2,1)} async-done(((bf16[64,2,2048]{2,0,1:T(8,128)(2,1)}), bf16[64,2,1024]{2,0,1:T(8,128)(2,1)}) %reduce-scatter.3.cloned.1.call-update) | async-done | bytes 262160 | tf_op jit(solution)/shard_map/reduce_scatter | solution.py:108
  48.1 1.0 convert_element_type.70
  49.3 2.5 %psum.36 = f32[64]{0:T(128)S(1)} all-reduce(f32[64]{0:T(128)S(1)} %get-tuple-element.14), channel_id=1, replica_groups=mesh['ep'=16,'tp'=2] {'tp'}, use_global_device_ids=true, to_apply=%region_4.0 | all-reduce | flops 64 | bytes 512 | tf_op jit(solution)/shard_map/psum | solution.py:120
  53.4 2.3 %all_gather.6 = bf16[64,2048]{1,0:T(8,128)(2,1)S(1)} all-gather(bf16[64,1024]{1,0:T(8,128)(2,1)} %fusion.43), channel_id=1, replica_groups=mesh['ep'=16,'tp'=2] {'tp'}, dimensions={1}, use_global_device_ids=true | all-gather | bytes 393216 | tf_op jit(solution)/shard_map/all_gather | solution.py:137
  56.2 41.0 %all_to_all.29 = bf16[16,16,2048]{2,1,0:T(8,128)(2,1)S(1)} all-to-all(bf16[16,16,2048]{2,1,0:T(8,128)(2,1)S(1)} %bitcast.74), channel_id=1, replica_groups=mesh['ep'=16,'tp'=2] {'ep'}, dimensions={0} | all-to-all | bytes 2097152 | tf_op jit(solution)/shard_map/all_to_all | solution.py:153
  97.2 1.0 copy-done.9
  98.9 4.2 %convolution_convert_fusion = bf16[256,2048]{1,0:T(8,128)(2,1)} fusion(bf16[1,512,2048]{2,1,0:T(8,128)(2,1)S(1)} %copy-done, bf16[256,2048]{1,0:T(8,128)(2,1)} %bitcast.79, bf16[1,2048,512]{2,1,0:T(8,128)(2,1)} %param.45, f32[256,512]{1,0:T(8,128)S(1)} %fusion.5), kind=kOutput, calls=%fused_computation.1 | convolution fusion | flops 1075052544 | bytes 6815744 | tf_op jit(solution)/shard_map/dot_general | solution.py:160
  103.1 3.8 %copy.77 = f32[64,64,64]{2,1,0:T(8,128)} copy(f32[64,64,64]{0,2,1:T(8,128)} %copy-done.2) | data formatting | bytes 2097152
  106.9 3.8 %copy.78 = f32[64,64,64]{2,1,0:T(8,128)} copy(f32[64,64,64]{0,2,1:T(8,128)} %copy-done.1) | data formatting | bytes 2097152
  111.7 3.3 %all-reduce = (f32[64,20]{0,1:T(8,128)S(1)}, f32[64]{0:T(128)S(1)}) all-reduce(f32[64,20]{0,1:T(8,128)S(1)} %fusion.44, f32[64]{0:T(128)S(1)} %convolution_bitcast_fusion), channel_id=1, replica_groups=mesh['ep'=16,'tp'=2] {'tp'}, use_global_device_ids=true, to_apply=%region_5.0 | all-reduce | flops 1344 | bytes 10752 | tf_op jit(solution)/shard_map/psum | solution.py:125
  115.1 3.4 %all-gather.2.cloned.1.call-done = bf16[1024,1024]{1,0:T(8,128)(2,1)} async-done(((bf16[64,1024]{1,0:T(8,128)(2,1)}), bf16[1024,1024]{1,0:T(8,128)(2,1)}) %all-gather.2.cloned.1.call-update) | async-done | bytes 2097168 | tf_op jit(solution)/shard_map/all_gather | solution.py:168
  118.5 2.4 %convolution_convert_fusion.4 = bf16[1024,128]{0,1:T(8,128)(2,1)S(1)} fusion(bf16[1024,1024]{1,0:T(8,128)(2,1)} %all-gather.2.cloned.1.call-done, bf16[1024,128]{1,0:T(8,128)(2,1)S(1)} %copy-done.12), kind=kOutput, calls=%fused_computation.17 | convolution fusion | flops 268566528 | bytes 2621440 | tf_op jit(solution)/shard_map/dot_general | solution.py:52
  120.9 7.1 %reduce-scatter.5.cloned.1.call-done = bf16[256,1024]{1,0:T(8,128)(2,1)} async-done(((bf16[256,2048]{1,0:T(8,128)(2,1)}), bf16[256,1024]{1,0:T(8,128)(2,1)}) %reduce-scatter.5.cloned.1.call-update) | async-done | bytes 524304 | tf_op jit(solution)/shard_map/reduce_scatter | solution.py:161
  128.0 6.8 %all-to-all-start.1 = ((bf16[16,16,1024]{2,1,0:T(8,128)(2,1)}), bf16[16,16,1024]{2,1,0:T(8,128)(2,1)S(1)}, u32[]{:S(2)}, u32[]{:S(2)}) async-start(bf16[16,16,1024]{2,1,0:T(8,128)(2,1)} %bitcast.80), calls=%async_computation.3 | async-start | bytes 1048576 | tf_op jit(solution)/shard_map/all_to_all | solution.py:163
  134.9 2.4 %convolution_convert_fusion.5 = bf16[1024,128]{0,1:T(8,128)(2,1)S(1)} fusion(bf16[1024,1024]{1,0:T(8,128)(2,1)} %all-gather.2.cloned.1.call-done, bf16[1024,128]{1,0:T(8,128)(2,1)S(1)} %copy-done.13), kind=kOutput, calls=%fused_computation.18 | convolution fusion | flops 268566528 | bytes 2621440 | tf_op jit(solution)/shard_map/dot_general | solution.py:51
  138.2 20.0 %all-reduce.3.cloned.1.call-done = bf16[1024,256]{0,1:T(8,128)(2,1)} async-done(((bf16[1024,256]{0,1:T(8,128)(2,1)}), bf16[1024,256]{0,1:T(8,128)(2,1)}) %all-reduce.3.cloned.1.call-update) | async-done | bytes 524304 | tf_op jit(solution)/shard_map/psum | solution.py:170
  158.2 1.1 convert_element_type.84
  160.3 6.8 %all-to-all-start.2 = ((bf16[16,64,128]{2,1,0:T(8,128)(2,1)}), bf16[16,64,128]{2,1,0:T(8,128)(2,1)S(1)}, u32[]{:S(2)}, u32[]{:S(2)}) async-start(bf16[16,64,128]{2,1,0:T(8,128)(2,1)} %bitcast.19), calls=%async_computation.4 | async-start | bytes 524288 | tf_op jit(solution)/shard_map/all_to_all | solution.py:175
  167.3 0.9 gather_fusion
  169.2 8.2 %all-to-all-done.2 = bf16[16,64,128]{2,1,0:T(8,128)(2,1)S(1)} async-done(((bf16[16,64,128]{2,1,0:T(8,128)(2,1)}), bf16[16,64,128]{2,1,0:T(8,128)(2,1)S(1)}, u32[]{:S(2)}, u32[]{:S(2)}) %all-to-all-start.2) | async-done | bytes 262176 | tf_op jit(solution)/shard_map/all_to_all | solution.py:175
  177.5 3.7 %fusion.14 = bf16[64,1024]{1,0:T(8,128)(2,1)} fusion(bf16[2048,1024]{1,0:T(8,128)(2,1)} %param.49, f32[64,1024]{1,0:T(8,128)S(1)} %multiply_reduce_fusion, bf16[64,1024]{1,0:T(8,128)(2,1)S(1)} %get-tuple-element.15, f32[64]{0:T(128)S(1)} %add_divide_fusion, bf16[16,64,128]{2,1,0:T(8,128)(2,1)S(1)} %all-to-all-done.2), kind=kOutput, calls=%fused_computation.21 | convolution fusion | flops 268763136 | bytes 4980992 | tf_op jit(solution)/shard_map/dot_general | solution.py:176
  (101 shorter events, 9.5 us)
Async XLA Ops:
  7.2 91.7 %copy-start = (bf16[1,512,2048]{2,1,0:T(8,128)(2,1)S(1)}, bf16[1,512,2048]{2,1,0:T(8,128)(2,1)}, u32[]{:S(2)}) copy-start(bf16[1,512,2048]{2,1,0:T(8,128)(2,1)} %param.46) | copy-start | bytes 6291460
  7.2 40.9 %reduce-scatter.3.cloned.1.call-start = ((), (), s32[]{:S(2)}) async-start(), calls=%async_computation.5 | async-start | bytes 786432 | tf_op jit(solution)/shard_map/reduce_scatter | solution.py:108
  10.7 3.4 %copy-start.6 = (bf16[64,1024]{1,0:T(8,128)(2,1)S(1)}, bf16[64,1024]{1,0:T(8,128)(2,1)}, u32[]{:S(2)}) copy-start(bf16[64,1024]{1,0:T(8,128)(2,1)} %param.25) | copy-start | bytes 393220
  10.7 6.2 %copy-start.18 = (f32[2048]{0:T(1024)S(1)}, f32[2048]{0:T(1024)}, u32[]{:S(2)}) copy-start(f32[2048]{0:T(1024)} %param.28) | copy-start | bytes 24580
  10.7 8.0 %copy-start.21 = (f32[64]{0:T(128)S(1)}, f32[64]{0:T(128)}, u32[]{:S(2)}) copy-start(f32[64]{0:T(128)} %param.32) | copy-start | bytes 772
  10.7 9.1 %copy-start.7 = (f32[64,64,16]{1,2,0:T(8,128)S(1)}, f32[64,64,16]{1,2,0:T(8,128)}, u32[]{:S(2)}) copy-start(f32[64,64,16]{1,2,0:T(8,128)} %param.34) | copy-start | bytes 786436
  10.7 9.1 %copy-start.8 = (f32[64,64,16]{1,2,0:T(8,128)S(1)}, f32[64,64,16]{1,2,0:T(8,128)}, u32[]{:S(2)}) copy-start(f32[64,64,16]{1,2,0:T(8,128)} %param.33) | copy-start | bytes 786436
  19.8 5.0 %copy-start.3 = (f32[64,64,64]{0,2,1:T(8,128)S(1)}, f32[64,64,64]{0,2,1:T(8,128)}, u32[]{:S(2)}) copy-start(f32[64,64,64]{0,2,1:T(8,128)} %copy.64) | copy-start | bytes 3145732
  19.8 5.0 %copy-start.4 = (f32[64,64,64]{0,2,1:T(8,128)S(1)}, f32[64,64,64]{0,2,1:T(8,128)}, u32[]{:S(2)}) copy-start(f32[64,64,64]{0,2,1:T(8,128)} %copy.63) | copy-start | bytes 3145732
  24.8 3.3 %copy-start.2 = (f32[64,64,64]{0,2,1:T(8,128)}, f32[64,64,64]{0,2,1:T(8,128)S(1)}, u32[]{:S(2)}) copy-start(f32[64,64,64]{0,2,1:T(8,128)S(1)} %bitcast_add_fusion.1) | copy-start | bytes 3145732
  24.8 3.3 %copy-start.11 = (f32[64,16,64]{2,1,0:T(8,128)S(1)}, f32[64,16,64]{2,1,0:T(8,128)}, u32[]{:S(2)}) copy-start(f32[64,16,64]{2,1,0:T(8,128)} %param.35) | copy-start | bytes 786436
  28.0 3.9 %copy-start.1 = (f32[64,64,64]{0,2,1:T(8,128)}, f32[64,64,64]{0,2,1:T(8,128)S(1)}, u32[]{:S(2)}) copy-start(f32[64,64,64]{0,2,1:T(8,128)S(1)} %bitcast_add_fusion) | copy-start | bytes 3145732
  28.0 1.9 %copy-start.10 = (f32[64,16,64]{2,1,0:T(8,128)S(1)}, f32[64,16,64]{2,1,0:T(8,128)}, u32[]{:S(2)}) copy-start(f32[64,16,64]{2,1,0:T(8,128)} %param.36) | copy-start | bytes 786436
  30.0 2.1 %copy-start.14 = (f32[1024]{0:T(1024)S(1)}, f32[1024]{0:T(1024)}, u32[]{:S(2)}) copy-start(f32[1024]{0:T(1024)} %param.37) | copy-start | bytes 12292
  32.1 3.5 %copy-start.5 = (bf16[1024,2048]{1,0:T(8,128)(2,1)S(1)}, bf16[1024,2048]{1,0:T(8,128)(2,1)}, u32[]{:S(2)}) copy-start(bf16[1024,2048]{1,0:T(8,128)(2,1)} %param.38) | copy-start | bytes 12582916
  35.6 1.9 %copy-start.19 = (f32[2048]{0:T(1024)S(1)}, f32[2048]{0:T(1024)}, u32[]{:S(2)}) copy-start(f32[2048]{0:T(1024)} %param.29) | copy-start | bytes 24580
  35.6 1.9 %copy-start.16 = (s32[64,2]{0,1:T(2,128)S(1)}, s32[64,2]{0,1:T(2,128)}, u32[]{:S(2)}) copy-start(s32[64,2]{0,1:T(2,128)} %param.43) | copy-start | bytes 1540
  37.4 81.1 %all-gather.2.cloned.1.call-start = ((), (), s32[]{:S(2)}) async-start(), calls=%async_computation.7 | async-start | bytes 2228224 | tf_op jit(solution)/shard_map/all_gather | solution.py:168
  52.5 75.5 %reduce-scatter.5.cloned.1.call-start = ((), (), s32[]{:S(2)}) async-start(), calls=%async_computation.6 | async-start | bytes 1572864 | tf_op jit(solution)/shard_map/reduce_scatter | solution.py:161
  53.3 44.9 %copy-start.20 = (bf16[1,2048,512]{2,1,0:T(8,128)(2,1)S(1)}, bf16[1,2048,512]{2,1,0:T(8,128)(2,1)}, u32[]{:S(2)}) copy-start(bf16[1,2048,512]{2,1,0:T(8,128)(2,1)} %param.44) | copy-start | bytes 6291460
  97.2 1.0 copy-start.9
  106.9 4.0 %copy-start.17 = (bf16[2048,4]{0,1:T(4,128)(2,1)S(1)}, bf16[2048,4]{0,1:T(4,128)(2,1)}, u32[]{:S(2)}) copy-start(bf16[2048,4]{0,1:T(4,128)(2,1)} %param.40) | copy-start | bytes 49156
  106.9 4.0 %copy-start.15 = (bf16[2048,16]{0,1:T(8,128)(2,1)S(1)}, bf16[2048,16]{0,1:T(8,128)(2,1)}, u32[]{:S(2)}) copy-start(bf16[2048,16]{0,1:T(8,128)(2,1)} %param.41) | copy-start | bytes 196612
  106.9 4.1 %dynamic-slice-start = ((f32[2048]{0:T(1024)}, s32[]{:T(128)}), f32[1024]{0:T(1024)S(1)}, s32[]{:S(2)}) async-start(f32[2048]{0:T(1024)} %param.42, s32[]{:T(128)} %select_n.30), calls=%async_computation.9 | async-start | bytes 8704 | tf_op jit(solution)/shard_map/dynamic_slice | solution.py:88
  106.9 11.6 %copy-start.12 = (bf16[1024,128]{1,0:T(8,128)(2,1)S(1)}, bf16[1024,128]{1,0:T(8,128)(2,1)}, u32[]{:S(2)}) copy-start(bf16[1024,128]{1,0:T(8,128)(2,1)} %param.48) | copy-start | bytes 786436
  111.0 23.9 %copy-start.13 = (bf16[1024,128]{1,0:T(8,128)(2,1)S(1)}, bf16[1024,128]{1,0:T(8,128)(2,1)}, u32[]{:S(2)}) copy-start(bf16[1024,128]{1,0:T(8,128)(2,1)} %param.47) | copy-start | bytes 786436
  128.0 32.3 %all-to-all-start.1 = ((bf16[16,16,1024]{2,1,0:T(8,128)(2,1)}), bf16[16,16,1024]{2,1,0:T(8,128)(2,1)S(1)}, u32[]{:S(2)}, u32[]{:S(2)}) async-start(bf16[16,16,1024]{2,1,0:T(8,128)(2,1)} %bitcast.80), calls=%async_computation.3 | async-start | bytes 1048576 | tf_op jit(solution)/shard_map/all_to_all | solution.py:163
  134.8 23.4 %all-reduce.3.cloned.1.call-start = ((), (), s32[]{:S(2)}) async-start(), calls=%async_computation.8 | async-start | bytes 1048576 | tf_op jit(solution)/shard_map/psum | solution.py:170
  160.3 17.1 %all-to-all-start.2 = ((bf16[16,64,128]{2,1,0:T(8,128)(2,1)}), bf16[16,64,128]{2,1,0:T(8,128)(2,1)S(1)}, u32[]{:S(2)}, u32[]{:S(2)}) async-start(bf16[16,64,128]{2,1,0:T(8,128)(2,1)} %bitcast.19), calls=%async_computation.4 | async-start | bytes 524288 | tf_op jit(solution)/shard_map/all_to_all | solution.py:175
Sparse Core Ops, SparseCore 0:
  37.6 10.4 reduce-scatter.2
  52.6 65.8 all-gather.1
  120.8 7.2 reduce-scatter.4
  138.3 19.8 all-reduce.2
where the time goes:
time: 188 us
  blocking collectives  51.7 us (28%)
  waiting for transfers between devices  49.1 us (26%)
  matrix products  30.9 us (16%)
  local copies, waits for them, and re-layouts  19.7 us (10%)
  between operations  14.3 us (8%)
  starting transfers between devices  13.8 us (7%)
  other arithmetic  8.23 us (4%)
    all_to_all x1, blocking collectives, shards(): lax.all_to_all(outgoing, 'ep', split_axis=0, concat_axis=0, tiled=True)  41 us
    psum x1, waiting for transfers between devices, shards(): lax.psum(partial_dense.astype(jnp.bfloat16), 'tp').astype(jnp.float32)  20 us
    unnamed x49, local copies, waits for them, and re-layouts  15.8 us
    reduce_scatter x1, waiting for transfers between devices, shards(): lax.psum_scatter(stacked.astype(jnp.bfloat16), 'tp', scatter_dimension=2,...  10.3 us
    all_to_all x1, waiting for transfers between devices, shards(): lax.all_to_all(inner_cols, 'ep', split_axis=0, concat_axis=1, tiled=True)  8.24 us
    reduce_scatter x1, waiting for transfers between devices, shards(): lax.psum_scatter(part_out.astype(jnp.bfloat16), 'tp', scatter_dimension=1...  7.08 us
    all_to_all x1, starting transfers between devices, shards(): lax.all_to_all(inner_cols, 'ep', split_axis=0, concat_axis=1, tiled=True)  6.83 us
    all_to_all x1, starting transfers between devices, shards(): lax.all_to_all(finished, 'ep', split_axis=0, concat_axis=0, tiled=True)  6.79 us
  transfers between devices with their start and end apart: 6, of which 5 were waited for; matrix products, arithmetic and copies ran while one was open for 13% of the time, Pallas kernels for 0%

commit v1 on v0

--- a/solution.py
+++ b/solution.py
@@ -167,7 +167,11 @@
     partial_dense = pair_product(
         lax.all_gather(hnorm, "ep", axis=0, tiled=True), shared_gate_weight, shared_up_weight
     )
-    dense_sum = lax.psum(partial_dense.astype(jnp.bfloat16), "tp").astype(jnp.float32)
+
+    def assign_the_scenes(v0):
+        return jnp.sum(lax.all_gather(v0, "tp"), axis=0)
+
+    dense_sum = assign_the_scenes(partial_dense.astype(jnp.bfloat16)).astype(jnp.float32)
     dense_cols = shared_gate_weight.shape[1]
     inner_cols = (jax.nn.silu(dense_sum[:, :dense_cols]) * dense_sum[:, dense_cols:]).astype(
         jnp.bfloat16

time: 188 us -> 174 us (0.926)
  waiting for transfers between devices: 49.1 us -> 35.9 us
  starting transfers between devices: 13.8 us -> 10.9 us
    psum x1 -> x0, waiting for transfers between devices: 20 us -> none  [shards(): lax.psum(partial_dense.astype(jnp.bfloat16), 'tp').astype(jnp.float32)]
    reduce_scatter x1, waiting for transfers between devices: 7.08 us -> 0.87 us  [shards(): lax.psum_scatter(part_out.astype(jnp.bfloat16), 'tp', scatter_dimension=1...]
    all_to_all x1, waiting for transfers between devices: 0.01 us -> 5.93 us  [shards(): lax.all_to_all(finished, 'ep', split_axis=0, concat_axis=0, tiled=True)]
    all_gather x0 -> x1, waiting for transfers between devices: none -> 4.68 us  [assign_the_scenes(): return jnp.sum(lax.all_gather(v0, 'tp'), axis=0)]
    all_gather x1, waiting for transfers between devices: 3.41 us -> 6.93 us  [shards(): lax.all_gather(hnorm, 'ep', axis=0, tiled=True)]
    all_to_all x1, starting transfers between devices: 6.83 us -> 3.99 us  [shards(): lax.all_to_all(inner_cols, 'ep', split_axis=0, concat_axis=1, tiled=True)]
    reduce_sum x0 -> x1, other arithmetic: none -> 2.37 us  [assign_the_scenes(): return jnp.sum(lax.all_gather(v0, 'tp'), axis=0)]
    unnamed x49 -> x50, local copies, waits for them, and re-layouts: 15.8 us -> 16 us
  transfers between devices with their start and end apart: 6 -> 6, of which waited for: 5 -> 6; matrix products, arithmetic and copies ran while one was open for 13% -> 15% of each run, Pallas kernels for 0% -> 0%
where the time goes in v1:
time: 174 us; the launch traced here: 173 us
  blocking collectives  51.9 us (30%)
  waiting for transfers between devices  35.9 us (21%)
  matrix products  30 us (17%)
  local copies, waits for them, and re-layouts  21 us (12%)
  between operations  14.3 us (8%)
  starting transfers between devices  10.9 us (6%)
  other arithmetic  8.75 us (5%)
    all_to_all x1, blocking collectives, shards(): lax.all_to_all(outgoing, 'ep', split_axis=0, concat_axis=0, tiled=True)  41.1 us
    unnamed x50, local copies, waits for them, and re-layouts  16 us
    reduce_scatter x1, waiting for transfers between devices, shards(): lax.psum_scatter(stacked.astype(jnp.bfloat16), 'tp', scatter_dimension=2,...  10.3 us
    all_to_all x1, waiting for transfers between devices, shards(): lax.all_to_all(inner_cols, 'ep', split_axis=0, concat_axis=1, tiled=True)  7.1 us
    all_gather x1, waiting for transfers between devices, shards(): lax.all_gather(hnorm, 'ep', axis=0, tiled=True)  6.93 us
    all_to_all x1, starting transfers between devices, shards(): lax.all_to_all(finished, 'ep', split_axis=0, concat_axis=0, tiled=True)  6.79 us
    all_to_all x1, waiting for transfers between devices, shards(): lax.all_to_all(finished, 'ep', split_axis=0, concat_axis=0, tiled=True)  5.93 us
    dot_general x1, matrix products, state_step(): jnp.einsum('tgc,gpc->tgp', grouped, bbar_re, precision=PRECISION_MAX)  4.93 us
  transfers between devices with their start and end apart: 6, of which 6 were waited for; matrix products, arithmetic and copies ran while one was open for 15% of the time, Pallas kernels for 0%

profile of v1, /device:TPU:0, one launch (start us, length us, event | category | flops | bytes accessed | tf_op | source)
XLA Modules:
  0.0 172.8 jit_solution(12865813921069355237)
XLA Ops:
  7.2 3.5 %copy.99 = f32[64,64,64]{0,2,1:T(8,128)} copy(f32[64,64,64]{2,1,0:T(8,128)} %param.27) | data formatting | bytes 2097152 | tf_op args[2]
  10.7 3.4 %copy.98 = f32[64,64,64]{0,2,1:T(8,128)} copy(f32[64,64,64]{2,1,0:T(8,128)} %param.26) | data formatting | bytes 2097152 | tf_op args[1]
  14.3 2.6 %psum.28 = f32[64]{0:T(128)S(1)} all-reduce(f32[64]{0:T(128)S(1)} %fusion.31), channel_id=1, replica_groups=mesh['ep'=16,'tp'=2] {'tp'}, use_global_device_ids=true, to_apply=%region_1.0 | all-reduce | flops 64 | bytes 512 | tf_op jit(solution)/shard_map/psum | solution.py:91
  17.7 1.1 copy.100
  18.8 1.0 fusion.70
  19.8 4.9 %bitcast_add_fusion.1 = f32[64,64,64]{0,2,1:T(8,128)S(1)} fusion(f32[64,64,64]{0,2,1:T(8,128)} %copy.99, f32[64,64,64]{0,2,1:T(8,128)} %copy.98, bf16[64,64,16]{0,2,1:T(8,128)(2,1)S(1)} %bitcast.79, f32[64,64]{1,0:T(8,128)S(1)} %get-tuple-element.23, f32[64,64]{1,0:T(8,128)S(1)} %get-tuple-element.24, f32[64,64,16]{1,2,0:T(8,128)S(1)} %copy-done.8, ...), kind=kOutput, calls=%fused_computation.13 | convolution fusion | flops 51576832 | bytes 3866624 | tf_op jit(solution)/shard_map/tgc,gpc->tgp/dot_general | solution.py:38
  24.8 3.2 %bitcast_add_fusion = f32[64,64,64]{0,2,1:T(8,128)S(1)} fusion(f32[64,64,64]{0,2,1:T(8,128)S(1)} %copy-done.4, f32[64,64,64]{0,2,1:T(8,128)S(1)} %copy-done.3, bf16[64,64,16]{0,2,1:T(8,128)(2,1)S(1)} %bitcast.80, f32[64,64]{1,0:T(8,128)S(1)} %get-tuple-element.23, f32[64,64]{1,0:T(8,128)S(1)} %get-tuple-element.24, f32[64,64,16]{1,2,0:T(8,128)S(1)} %copy-done.9, ...), kind=kOutput, calls=%fused_computation.12 | convolution fusion | flops 51576832 | bytes 3866624 | tf_op jit(solution)/shard_map/tgc,gpc->tgp/dot_general | solution.py:39
  28.1 1.9 %fusion.79 = f32[64,64,16]{1,2,0:T(8,128)S(1)} fusion(f32[64,64,64]{0,2,1:T(8,128)S(1)} %bitcast_add_fusion.1, f32[64,16,64]{2,1,0:T(8,128)S(1)} %copy-done.11), kind=kOutput, calls=%fused_computation.125 | convolution fusion | flops 50331648 | bytes 1572864 | tf_op jit(solution)/shard_map/dor,zdr->zdo/dot_general | solution.py:42
  30.0 1.9 %convolution_subtract_fusion = f32[64,64,16]{1,2,0:T(8,128)S(1)} fusion(f32[64,64,16]{1,2,0:T(8,128)S(1)} %fusion.79, f32[64,64,64]{0,2,1:T(8,128)S(1)} %bitcast_add_fusion, f32[64,16,64]{2,1,0:T(8,128)S(1)} %copy-done.10), kind=kOutput, calls=%fused_computation.15 | convolution fusion | flops 50397184 | bytes 1835008 | tf_op jit(solution)/shard_map/dor,zdr->zdo/dot_general | solution.py:43
  32.1 3.3 %fusion.1 = bf16[64,1,2048]{2,0,1:T(8,128)(2,1)S(1)} fusion(bf16[1024,2048]{1,0:T(8,128)(2,1)} %param.39, f32[64,1024]{1,0:T(8,128)S(1)} %copy.105, f32[1024]{0:T(1024)S(1)} %copy-done.14, f32[1024]{0:T(1024)S(1)} %dynamic_slice.15, f32[64]{0:T(128)S(1)} %add_rsqrt_fusion.1, bf16[64,1024]{1,0:T(8,128)(2,1)S(1)} %copy-done.7), kind=kOutput, calls=%fused_computation.6 | convolution fusion | flops 269615104 | bytes 4858112 | tf_op jit(solution)/shard_map/dot_general | solution.py:106
  35.6 1.0 fusion
  37.8 10.3 %reduce-scatter.3.cloned.1.call-done = bf16[64,2,1024]{2,0,1:T(8,128)(2,1)} async-done(((bf16[64,2,2048]{2,0,1:T(8,128)(2,1)}), bf16[64,2,1024]{2,0,1:T(8,128)(2,1)}) %reduce-scatter.3.cloned.1.call-update) | async-done | bytes 262160 | tf_op jit(solution)/shard_map/reduce_scatter | solution.py:108
  48.1 1.0 convert_element_type.79
  49.3 2.5 %psum.29 = f32[64]{0:T(128)S(1)} all-reduce(f32[64]{0:T(128)S(1)} %get-tuple-element.20), channel_id=1, replica_groups=mesh['ep'=16,'tp'=2] {'tp'}, use_global_device_ids=true, to_apply=%region_4.0 | all-reduce | flops 64 | bytes 512 | tf_op jit(solution)/shard_map/psum | solution.py:120
  53.4 2.3 %all_gather.10 = bf16[64,2048]{1,0:T(8,128)(2,1)S(1)} all-gather(bf16[64,1024]{1,0:T(8,128)(2,1)} %fusion.45), channel_id=1, replica_groups=mesh['ep'=16,'tp'=2] {'tp'}, dimensions={1}, use_global_device_ids=true | all-gather | bytes 393216 | tf_op jit(solution)/shard_map/all_gather | solution.py:137
  56.2 41.1 %all_to_all.29 = bf16[16,16,2048]{2,1,0:T(8,128)(2,1)S(1)} all-to-all(bf16[16,16,2048]{2,1,0:T(8,128)(2,1)S(1)} %bitcast.78), channel_id=1, replica_groups=mesh['ep'=16,'tp'=2] {'ep'}, dimensions={0} | all-to-all | bytes 2097152 | tf_op jit(solution)/shard_map/all_to_all | solution.py:153
  97.3 1.5 fusion.5
  98.8 4.0 %convolution_convert_fusion = bf16[256,2048]{1,0:T(8,128)(2,1)} fusion(bf16[1,512,2048]{2,1,0:T(8,128)(2,1)S(1)} %copy-done, bf16[256,2048]{1,0:T(8,128)(2,1)S(1)} %bitcast.83, bf16[1,2048,512]{2,1,0:T(8,128)(2,1)} %param.45, f32[256,512]{1,0:T(8,128)} %fusion.5), kind=kOutput, calls=%fused_computation.1 | convolution fusion | flops 1075052544 | bytes 6815744 | tf_op jit(solution)/shard_map/dot_general | solution.py:160
  102.9 3.8 %copy.114 = f32[64,64,64]{2,1,0:T(8,128)} copy(f32[64,64,64]{0,2,1:T(8,128)} %copy-done.2) | data formatting | bytes 2097152
  106.6 3.8 %copy.115 = f32[64,64,64]{2,1,0:T(8,128)} copy(f32[64,64,64]{0,2,1:T(8,128)} %copy-done.1) | data formatting | bytes 2097152
  110.7 6.9 %all-gather.3.cloned.1.call-done = bf16[1024,1024]{1,0:T(8,128)(2,1)} async-done(((bf16[64,1024]{1,0:T(8,128)(2,1)}), bf16[1024,1024]{1,0:T(8,128)(2,1)}) %all-gather.3.cloned.1.call-update) | async-done | bytes 2097168 | tf_op jit(solution)/shard_map/all_gather | solution.py:168
  117.6 2.6 %fusion.14 = bf16[1,1024,128]{1,2,0:T(8,128)(2,1)S(1)} fusion(bf16[1024,1024]{1,0:T(8,128)(2,1)} %all-gather.3.cloned.1.call-done, bf16[1024,128]{1,0:T(8,128)(2,1)S(1)} %copy-done.12), kind=kOutput, calls=%fused_computation.20 | convolution fusion | flops 268566528 | bytes 2621440 | tf_op jit(solution)/shard_map/dot_general | solution.py:52
  121.1 1.0 copy.110
  122.9 3.3 %all-reduce = (f32[64,20]{0,1:T(8,128)S(1)}, f32[64]{0:T(128)S(1)}) all-reduce(f32[64,20]{0,1:T(8,128)S(1)} %fusion.46, f32[64]{0:T(128)S(1)} %convolution_bitcast_fusion), channel_id=1, replica_groups=mesh['ep'=16,'tp'=2] {'tp'}, use_global_device_ids=true, to_apply=%region_5.0 | all-reduce | flops 1344 | bytes 10752 | tf_op jit(solution)/shard_map/psum | solution.py:125
  127.1 6.8 %all-to-all-start.1 = ((bf16[16,16,1024]{2,1,0:T(8,128)(2,1)}), bf16[16,16,1024]{2,1,0:T(8,128)(2,1)S(1)}, u32[]{:S(2)}, u32[]{:S(2)}) async-start(bf16[16,16,1024]{2,1,0:T(8,128)(2,1)} %bitcast.84), calls=%async_computation.3 | async-start | bytes 1048576 | tf_op jit(solution)/shard_map/all_to_all | solution.py:163
  134.0 4.7 %all-gather.5.cloned.1.call-done = bf16[2,1024,256]{2,1,0:T(8,128)(2,1)} async-done(((bf16[1,1024,256]{2,1,0:T(8,128)(2,1)}), bf16[2,1024,256]{2,1,0:T(8,128)(2,1)}) %all-gather.5.cloned.1.call-update) | async-done | bytes 1048592 | tf_op jit(solution)/shard_map/all_gather | solution.py:172
  138.7 2.4 %reduce_sum.102 = bf16[1024,256]{1,0:T(8,128)(2,1)} reduce(bf16[2,1024,256]{2,1,0:T(8,128)(2,1)} %all-gather.5.cloned.1.call-done, bf16[]{:T(256)} %constant.64.clone.1), dimensions={0}, to_apply=%region_18.19 | reduce | flops 262144 | bytes 1572866 | tf_op jit(solution)/shard_map/reduce_sum | solution.py:172
  141.1 1.2 copy.118
  143.5 5.9 %all-to-all-done.1 = bf16[16,16,1024]{2,1,0:T(8,128)(2,1)S(1)} async-done(((bf16[16,16,1024]{2,1,0:T(8,128)(2,1)}), bf16[16,16,1024]{2,1,0:T(8,128)(2,1)S(1)}, u32[]{:S(2)}, u32[]{:S(2)}) %all-to-all-start.1) | async-done | bytes 524320 | tf_op jit(solution)/shard_map/all_to_all | solution.py:163
  149.4 4.0 %all-to-all-start.2 = ((bf16[16,64,128]{2,1,0:T(8,128)(2,1)}), bf16[16,64,128]{2,1,0:T(8,128)(2,1)S(1)}, u32[]{:S(2)}, u32[]{:S(2)}) async-start(bf16[16,64,128]{2,1,0:T(8,128)(2,1)} %bitcast.21), calls=%async_computation.4 | async-start | bytes 524288 | tf_op jit(solution)/shard_map/all_to_all | solution.py:179
  155.4 7.1 %all-to-all-done.2 = bf16[16,64,128]{2,1,0:T(8,128)(2,1)S(1)} async-done(((bf16[16,64,128]{2,1,0:T(8,128)(2,1)}), bf16[16,64,128]{2,1,0:T(8,128)(2,1)S(1)}, u32[]{:S(2)}, u32[]{:S(2)}) %all-to-all-start.2) | async-done | bytes 262176 | tf_op jit(solution)/shard_map/all_to_all | solution.py:179
  162.5 3.7 %fusion.16 = bf16[64,1024]{1,0:T(8,128)(2,1)} fusion(bf16[2048,1024]{1,0:T(8,128)(2,1)} %param.49, f32[64,1024]{1,0:T(8,128)S(1)} %multiply_reduce_fusion, bf16[64,1024]{1,0:T(8,128)(2,1)S(1)} %get-tuple-element.21, f32[64]{0:T(128)S(1)} %add_divide_fusion, bf16[16,64,128]{2,1,0:T(8,128)(2,1)S(1)} %all-to-all-done.2), kind=kOutput, calls=%fused_computation.23 | convolution fusion | flops 268763136 | bytes 4980992 | tf_op jit(solution)/shard_map/dot_general | solution.py:180
  (104 shorter events, 10.6 us)
Async XLA Ops:
  7.2 91.6 %copy-start = (bf16[1,512,2048]{2,1,0:T(8,128)(2,1)S(1)}, bf16[1,512,2048]{2,1,0:T(8,128)(2,1)}, u32[]{:S(2)}) copy-start(bf16[1,512,2048]{2,1,0:T(8,128)(2,1)} %param.46) | copy-start | bytes 6291460
  7.2 40.9 %reduce-scatter.3.cloned.1.call-start = ((), (), s32[]{:S(2)}) async-start(), calls=%async_computation.5 | async-start | bytes 786432 | tf_op jit(solution)/shard_map/reduce_scatter | solution.py:108
  10.7 3.4 %copy-start.7 = (bf16[64,1024]{1,0:T(8,128)(2,1)S(1)}, bf16[64,1024]{1,0:T(8,128)(2,1)}, u32[]{:S(2)}) copy-start(bf16[64,1024]{1,0:T(8,128)(2,1)} %param.25) | copy-start | bytes 393220
  10.7 6.2 %copy-start.18 = (f32[2048]{0:T(1024)S(1)}, f32[2048]{0:T(1024)}, u32[]{:S(2)}) copy-start(f32[2048]{0:T(1024)} %param.28) | copy-start | bytes 24580
  10.7 8.0 %copy-start.21 = (f32[64]{0:T(128)S(1)}, f32[64]{0:T(128)}, u32[]{:S(2)}) copy-start(f32[64]{0:T(128)} %param.32) | copy-start | bytes 772
  10.7 9.1 %copy-start.8 = (f32[64,64,16]{1,2,0:T(8,128)S(1)}, f32[64,64,16]{1,2,0:T(8,128)}, u32[]{:S(2)}) copy-start(f32[64,64,16]{1,2,0:T(8,128)} %param.34) | copy-start | bytes 786436
  10.7 9.1 %copy-start.9 = (f32[64,64,16]{1,2,0:T(8,128)S(1)}, f32[64,64,16]{1,2,0:T(8,128)}, u32[]{:S(2)}) copy-start(f32[64,64,16]{1,2,0:T(8,128)} %param.33) | copy-start | bytes 786436
  19.8 5.0 %copy-start.3 = (f32[64,64,64]{0,2,1:T(8,128)S(1)}, f32[64,64,64]{0,2,1:T(8,128)}, u32[]{:S(2)}) copy-start(f32[64,64,64]{0,2,1:T(8,128)} %copy.99) | copy-start | bytes 3145732
  19.8 5.0 %copy-start.4 = (f32[64,64,64]{0,2,1:T(8,128)S(1)}, f32[64,64,64]{0,2,1:T(8,128)}, u32[]{:S(2)}) copy-start(f32[64,64,64]{0,2,1:T(8,128)} %copy.98) | copy-start | bytes 3145732
  24.8 3.3 %copy-start.2 = (f32[64,64,64]{0,2,1:T(8,128)}, f32[64,64,64]{0,2,1:T(8,128)S(1)}, u32[]{:S(2)}) copy-start(f32[64,64,64]{0,2,1:T(8,128)S(1)} %bitcast_add_fusion.1) | copy-start | bytes 3145732
  24.8 3.3 %copy-start.11 = (f32[64,16,64]{2,1,0:T(8,128)S(1)}, f32[64,16,64]{2,1,0:T(8,128)}, u32[]{:S(2)}) copy-start(f32[64,16,64]{2,1,0:T(8,128)} %param.35) | copy-start | bytes 786436
  28.0 3.9 %copy-start.1 = (f32[64,64,64]{0,2,1:T(8,128)}, f32[64,64,64]{0,2,1:T(8,128)S(1)}, u32[]{:S(2)}) copy-start(f32[64,64,64]{0,2,1:T(8,128)S(1)} %bitcast_add_fusion) | copy-start | bytes 3145732
  28.0 1.9 %copy-start.10 = (f32[64,16,64]{2,1,0:T(8,128)S(1)}, f32[64,16,64]{2,1,0:T(8,128)}, u32[]{:S(2)}) copy-start(f32[64,16,64]{2,1,0:T(8,128)} %param.36) | copy-start | bytes 786436
  30.0 2.1 %copy-start.14 = (f32[1024]{0:T(1024)S(1)}, f32[1024]{0:T(1024)}, u32[]{:S(2)}) copy-start(f32[1024]{0:T(1024)} %param.37) | copy-start | bytes 12292
  32.1 3.5 %copy-start.6 = (bf16[1024,2048]{1,0:T(8,128)(2,1)S(1)}, bf16[1024,2048]{1,0:T(8,128)(2,1)}, u32[]{:S(2)}) copy-start(bf16[1024,2048]{1,0:T(8,128)(2,1)} %param.38) | copy-start | bytes 12582916
  35.6 1.9 %copy-start.19 = (f32[2048]{0:T(1024)S(1)}, f32[2048]{0:T(1024)}, u32[]{:S(2)}) copy-start(f32[2048]{0:T(1024)} %param.29) | copy-start | bytes 24580
  35.6 1.9 %copy-start.16 = (s32[64,2]{0,1:T(2,128)S(1)}, s32[64,2]{0,1:T(2,128)}, u32[]{:S(2)}) copy-start(s32[64,2]{0,1:T(2,128)} %param.43) | copy-start | bytes 1540
  37.4 80.2 %all-gather.3.cloned.1.call-start = ((), (), s32[]{:S(2)}) async-start(), calls=%async_computation.7 | async-start | bytes 2228224 | tf_op jit(solution)/shard_map/all_gather | solution.py:168
  52.5 74.6 %reduce-scatter.5.cloned.1.call-start = ((), (), s32[]{:S(2)}) async-start(), calls=%async_computation.6 | async-start | bytes 1572864 | tf_op jit(solution)/shard_map/reduce_scatter | solution.py:161
  53.3 44.0 %copy-start.20 = (bf16[1,2048,512]{2,1,0:T(8,128)(2,1)S(1)}, bf16[1,2048,512]{2,1,0:T(8,128)(2,1)}, u32[]{:S(2)}) copy-start(bf16[1,2048,512]{2,1,0:T(8,128)(2,1)} %param.44) | copy-start | bytes 6291460
  102.8 35.9 %all-gather.5.cloned.1.call-start = ((), (), s32[]{:S(2)}) async-start(), calls=%async_computation.8 | async-start | bytes 1572864 | tf_op jit(solution)/shard_map/all_gather | solution.py:172
  106.6 4.0 %copy-start.17 = (bf16[2048,4]{0,1:T(4,128)(2,1)S(1)}, bf16[2048,4]{0,1:T(4,128)(2,1)}, u32[]{:S(2)}) copy-start(bf16[2048,4]{0,1:T(4,128)(2,1)} %param.40) | copy-start | bytes 49156
  106.6 4.0 %copy-start.15 = (bf16[2048,16]{0,1:T(8,128)(2,1)S(1)}, bf16[2048,16]{0,1:T(8,128)(2,1)}, u32[]{:S(2)}) copy-start(bf16[2048,16]{0,1:T(8,128)(2,1)} %param.41) | copy-start | bytes 196612
  106.6 11.0 %copy-start.12 = (bf16[1024,128]{1,0:T(8,128)(2,1)S(1)}, bf16[1024,128]{1,0:T(8,128)(2,1)}, u32[]{:S(2)}) copy-start(bf16[1024,128]{1,0:T(8,128)(2,1)} %param.48) | copy-start | bytes 786436
  110.5 9.8 %copy-start.13 = (bf16[1024,128]{1,0:T(8,128)(2,1)S(1)}, bf16[1024,128]{1,0:T(8,128)(2,1)}, u32[]{:S(2)}) copy-start(bf16[1024,128]{1,0:T(8,128)(2,1)} %param.47) | copy-start | bytes 786436
  117.6 2.6 %copy-start.5 = (bf16[1024,1024]{1,0:T(8,128)(2,1)S(1)}, bf16[1024,1024]{1,0:T(8,128)(2,1)}, u32[]{:S(2)}) copy-start(bf16[1024,1024]{1,0:T(8,128)(2,1)} %all-gather.3.cloned.1.call-done) | copy-start | bytes 6291460
  120.2 2.0 %dynamic-slice-start = ((f32[2048]{0:T(1024)}, s32[]{:T(128)}), f32[1024]{0:T(1024)S(1)}, s32[]{:S(2)}) async-start(f32[2048]{0:T(1024)} %param.42, s32[]{:T(128)} %select_n.30), calls=%async_computation.9 | async-start | bytes 8704 | tf_op jit(solution)/shard_map/dynamic_slice | solution.py:88
  127.1 22.3 %all-to-all-start.1 = ((bf16[16,16,1024]{2,1,0:T(8,128)(2,1)}), bf16[16,16,1024]{2,1,0:T(8,128)(2,1)S(1)}, u32[]{:S(2)}, u32[]{:S(2)}) async-start(bf16[16,16,1024]{2,1,0:T(8,128)(2,1)} %bitcast.84), calls=%async_computation.3 | async-start | bytes 1048576 | tf_op jit(solution)/shard_map/all_to_all | solution.py:163
  149.4 13.1 %all-to-all-start.2 = ((bf16[16,64,128]{2,1,0:T(8,128)(2,1)}), bf16[16,64,128]{2,1,0:T(8,128)(2,1)S(1)}, u32[]{:S(2)}, u32[]{:S(2)}) async-start(bf16[16,64,128]{2,1,0:T(8,128)(2,1)} %bitcast.21), calls=%async_computation.4 | async-start | bytes 524288 | tf_op jit(solution)/shard_map/all_to_all | solution.py:179
Sparse Core Ops, SparseCore 0:
  37.6 10.4 reduce-scatter.2
  52.6 64.9 all-gather.2
  119.9 7.1 reduce-scatter.4
  128.5 10.1 all-gather.4
